TPU v7x, 32 devices: a whole 2x2x4 slice. The times are simulated.
32 devices in a mesh: grp: 1, sp: 16 (over z, y, core), tp: 2 (over x).
Axes of the slice: x: 2, y: 2, z: 4, core: 2. Of those that a mesh axis runs over, the one named last changes fastest.
Arguments:
- residual: bfloat16 [8192, 2048], P(('grp', 'sp', 'tp')), may hold values from -6 to 6
- queries: bfloat16 [8192, 2048], P(('grp', 'sp'), 'tp'), may hold values from -200 to 200
- key_heads: bfloat16 [8192, 256], P(('grp', 'sp'), 'tp'), may hold values from -8 to 8
- value_heads: bfloat16 [8192, 256], P(('grp', 'sp'), 'tp'), may hold values from -6 to 6
- documents: int32 [8192], P(('grp', 'sp')), may hold values from 0 to 3, never falling along the last dimension, each value on 1 to 4096 neighbouring positions
- sink_logits: float32 [32], P('tp'), may hold values from 4 to 7
- out_weight: bfloat16 [2048, 2048], P('tp'), may hold values from -1 to 1
- norm_gain: bfloat16 [2048], replicated, may hold values from 0.099609375 to 1.8984375
- gate_weight: bfloat16 [2048, 5632], P('sp', 'tp'), may hold values from -0.125 to 0.125
- up_weight: bfloat16 [2048, 5632], P('sp', 'tp'), may hold values from -0.125 to 0.125
- down_weight: bfloat16 [2048, 5632], P('sp', 'tp'), may hold values from -0.078125 to 0.078125
Outputs:
- updated: bfloat16 [8192, 2048], P(('grp', 'sp', 'tp'))
Inputs may be any that keep to these rules, and one draw needn't show every extreme that they name: `documents`: document numbers never fall along the sequence.
All inputs are finite; a program needn't handle non-finite values.
Results may differ from a plain program's by a relative error of at most 0.012.
Values may be sent and summed in bfloat16 or wider, within the bound.
A program may use at most 128 MiB of HBM per device.

v0:
```python
import jax
import jax.numpy as jnp
from jax import lax
from jax.sharding import PartitionSpec as P

HD = 64
WINDOW = 128
epsilon = 1e-06
masked = -1e30


def padded(shard, sides, width):
    for axis, dim in sides:
        size, length = (lax.axis_size(axis), shard.shape[dim])
        up = [(i, (i + 1) % size) for i in range(size - 1)]
        down = [(j, i) for i, j in up]
        last = lax.slice_in_dim(shard, length - width, length, axis=dim)
        initial = lax.slice_in_dim(shard, 0, width, axis=dim)
        before = lax.ppermute(last, axis, up)
        after = lax.ppermute(initial, axis, down)
        shard = jnp.concatenate([before, shard, after], axis=dim)
    return shard


def on_device(
    residual,
    queries,
    key_heads,
    value_heads,
    documents,
    sink_logits,
    out_weight,
    norm_gain,
    gate_weight,
    up_weight,
    down_weight,
):
    tok_rows = queries.shape[0]
    kv_local = key_heads.shape[1] // HD
    q_local = queries.shape[1] // HD
    groups = q_local // kv_local
    own_docs = documents.astype(jnp.bfloat16)
    spread_keys, spread_values, spread_docs = (
        padded(key_heads, (("sp", 0),), WINDOW),
        padded(value_heads, (("sp", 0),), WINDOW),
        padded(own_docs, (("sp", 0),), WINDOW),
    )
    offset = lax.axis_index("sp") * tok_rows
    total_length = tok_rows * lax.axis_size("sp")
    query_pos = offset + jnp.arange(tok_rows, dtype=jnp.int32)
    key_pos = offset - WINDOW + jnp.arange(tok_rows + 2 * WINDOW, dtype=jnp.int32)
    allowed = (
        (jnp.abs(query_pos[:, None] - key_pos[None, :]) <= WINDOW)
        & (key_pos >= 0)[None, :]
        & (key_pos < total_length)[None, :]
        & (own_docs[:, None] == spread_docs[None, :])
    )
    query_block = queries.reshape(tok_rows, kv_local, groups, HD)
    key_block = spread_keys.reshape(-1, kv_local, HD)
    value_block = spread_values.reshape(-1, kv_local, HD)
    scores = jnp.einsum(
        "qkgd,jkd->kgqj", query_block, key_block, preferred_element_type=jnp.float32
    ) * HD ** (-0.5)
    scores = jnp.where(allowed[None, None], scores, masked)
    sink_table = sink_logits.reshape(kv_local, groups)[:, :, None]
    row_max = jnp.maximum(jnp.max(scores, axis=-1), sink_table)
    expo = jnp.exp(scores - row_max[..., None])
    total = jnp.sum(expo, axis=-1) + jnp.exp(sink_table - row_max)
    probs = (expo / total[..., None]).astype(jnp.bfloat16)
    mixed = jnp.einsum("kgqj,jkd->qkgd", probs, value_block, preferred_element_type=jnp.float32)
    attended = mixed.reshape(tok_rows, q_local * HD).astype(jnp.bfloat16)
    projected = lax.psum_scatter(
        jnp.dot(attended, out_weight, preferred_element_type=jnp.float32).astype(jnp.bfloat16),
        "tp",
        scatter_dimension=0,
        tiled=True,
    )
    middle = (
        residual.astype(jnp.float32) + lax.optimization_barrier(projected).astype(jnp.float32)
    ).astype(jnp.bfloat16)
    middle_wide = middle.astype(jnp.float32)
    scaled = middle_wide * lax.rsqrt(
        jnp.mean(middle_wide * middle_wide, axis=-1, keepdims=True) + epsilon
    )
    normed = (scaled * norm_gain.astype(jnp.float32)).astype(jnp.bfloat16)
    whole_gate, whole_up, whole_down = (
        lax.all_gather(gate_weight, "sp", axis=0, tiled=True),
        lax.all_gather(up_weight, "sp", axis=0, tiled=True),
        lax.all_gather(down_weight, "sp", axis=0, tiled=True),
    )
    row_piece = lax.all_gather(normed, "tp", axis=0, tiled=True)
    gate_value = jnp.dot(row_piece, whole_gate, preferred_element_type=jnp.float32)
    up_value = jnp.dot(row_piece, whole_up, preferred_element_type=jnp.float32)
    hidden = (jax.nn.silu(gate_value) * up_value).astype(jnp.bfloat16)
    mixer_out = lax.psum_scatter(
        lax.dot_general(
            hidden, whole_down, (((1,), (1,)), ((), ())), preferred_element_type=jnp.float32
        ).astype(jnp.bfloat16),
        "tp",
        scatter_dimension=0,
        tiled=True,
    )
    updated = middle.astype(jnp.float32) + 0.5 * lax.optimization_barrier(mixer_out).astype(
        jnp.float32
    )
    return updated.astype(jnp.bfloat16)


def solution(mesh):
    return jax.shard_map(
        on_device,
        mesh=mesh,
        in_specs=(
            P(("grp", "sp", "tp"), None),
            P(("grp", "sp"), "tp"),
            P(("grp", "sp"), "tp"),
            P(("grp", "sp"), "tp"),
            P(("grp", "sp")),
            P("tp"),
            P("tp", None),
            P(),
            P("sp", "tp"),
            P("sp", "tp"),
            P("sp", "tp"),
        ),
        out_specs=P(("grp", "sp", "tp"), None),
        check_vma=False,
    )
```

profile of v0, /device:TPU:0, one launch (start us, length us, event | category | flops | bytes accessed | tf_op | source)
XLA Modules:
  0.0 484.4 jit_solution(10772446977778538224)
XLA Ops:
  6.5 0.0 reduce-scatter.3.cloned.1.call-start
  6.5 0.7 convert_element_type.50
  7.2 2.4 collective-permute-start.2
  9.6 1.3 collective-permute-start.3
  10.9 0.8 fusion.16
  11.7 5.1 %collective-permute-start.4 = (bf16[128,128]{1,0:T(8,128)(2,1)S(1)}, bf16[128,128]{1,0:T(8,128)(2,1)S(1)}, u32[]{:S(2)}, u32[]{:S(2)}) collective-permute-start(bf16[128,128]{1,0:T(8,128)(2,1)S(1)} %get-tuple-element.5), channel_id=1, source_target_pairs={{0,2},{2,4},{4,6},{6,8},{8,10},{10,12},{12,14},{14,16},{16,18},{18... | collective-permute-start | bytes 98312 | tf_op jit(solution)/shard_map/ppermute | solution.py:19
  16.9 1.3 collective-permute-start.5
  18.2 0.8 fusion.17
  18.9 4.3 collective-permute-start
  23.3 1.5 copy.18
  24.8 0.7 max.17
  25.5 0.0 collective-permute-done.2
  25.5 1.3 collective-permute-start.1
  26.8 0.0 collective-permute-done.3
  26.8 1.0 fusion.9
  27.8 0.0 collective-permute-done.4
  27.8 0.0 collective-permute-done.5
  27.8 0.9 pad_maximum_fusion.1
  28.8 0.1 copy.17
  28.9 3.7 fusion.1
  32.7 0.0 copy-start
  32.7 0.1 broadcast_maximum_fusion
  32.7 0.0 copy-start.3
  32.7 5.2 %fusion = f32[2,8,512]{2,1,0:T(8,128)S(1)} fusion(f32[2,768,512,8]{2,1,3,0:T(8,128)S(1)} %get-tuple-element.12, f32[2,8,512]{2,1,0:T(8,128)S(1)} %broadcast_maximum_fusion, pred[512,768]{0,1:T(8,128)(4,1)S(1)} %fusion.9), kind=kLoop, calls=%fused_computation.3 | loop fusion | flops 25157632 | bytes 25624576 | tf_op jit(solution)/shard_map/reduce_sum | solution.py:68
  38.0 3.0 copy-done
  41.0 0.1 exponential_add_fusion
  41.1 0.0 collective-permute-done
  41.1 0.0 collective-permute-done.1
  41.1 0.0 copy-done.3
  41.2 0.1 copy.16
  41.3 0.0 copy-start.5
  41.3 12.0 %fusion.10 = bf16[2,64,8,512]{3,1,2,0:T(8,128)(2,1)S(1)} fusion(bf16[768,2,64,1]{0,2,3,1:T(8,128)(2,1)S(1)} %bitcast.37, f32[2,768,512,8]{2,1,3,0:T(8,128)} %copy-done, f32[2,8,512]{2,1,0:T(8,128)S(1)} %exponential_add_fusion, f32[2,8,512]{2,1,0:T(8,128)S(1)} %broadcast_maximum_fusion, pred[512,768]{0,1:T(8,128)(4,1)S(1)} %fusion.9), kind=kOutput, calls=%fused_computation.21 | convolution fusion | flops 837287936 | bytes 26869760 | tf_op jit(solution)/shard_map/kgqj,jkd->qkgd/dot_general | solution.py:70
  53.3 0.0 copy-done.5
  53.4 0.0 copy-start.4
  53.4 0.0 copy-start.1
  53.4 3.8 convolution_convert_fusion
  57.2 0.0 reduce-scatter.3.cloned.1.call-update
  57.2 0.0 all-gather.5.cloned.1.call-start
  57.2 0.0 copy-done.4
  57.3 37.5 %reduce-scatter.3.cloned.1.call-done = bf16[256,2048]{1,0:T(8,128)(2,1)} async-done(((bf16[512,2048]{1,0:T(8,128)(2,1)}), bf16[256,2048]{1,0:T(8,128)(2,1)}) %reduce-scatter.3.cloned.1.call-update) | async-done | bytes 1048592 | tf_op jit(solution)/shard_map/reduce_scatter | solution.py:72
  94.7 0.0 copy-done.1
  94.7 1.6 fusion.3
  96.4 2.6 fusion.5
  99.0 0.0 all-gather.5.cloned.1.call-update
  99.0 0.0 all-gather.7.cloned.1.call-start
  99.0 0.7 all-gather.7.cloned.1.call-update
  99.7 0.2 all-gather.11.cloned.1.call-start
  99.9 0.3 all-gather.11.cloned.1.call-update
  100.3 0.0 all-gather.9.cloned.1.call-start
  100.3 0.5 all-gather.9.cloned.1.call-update
  100.9 0.0 reduce-scatter.5.cloned.1.call-start
  100.9 31.3 %all-gather.5.cloned.1.call-done = bf16[512,2048]{1,0:T(8,128)(2,1)} async-done(((bf16[256,2048]{1,0:T(8,128)(2,1)}), bf16[512,2048]{1,0:T(8,128)(2,1)}) %all-gather.5.cloned.1.call-update) | async-done | bytes 2097168 | tf_op jit(solution)/shard_map/all_gather | solution.py:91
  132.2 96.3 %all-gather.7.cloned.1.call-done = bf16[2048,2816]{1,0:T(8,128)(2,1)} async-done(((bf16[128,2816]{1,0:T(8,128)(2,1)}), bf16[2048,2816]{1,0:T(8,128)(2,1)}) %all-gather.7.cloned.1.call-update) | async-done | bytes 11534352 | tf_op jit(solution)/shard_map/all_gather | solution.py:87
  228.5 12.5 %fusion.19 = f32[512,2816]{1,0:T(8,128)} fusion(bf16[512,2048]{1,0:T(8,128)(2,1)} %all-gather.5.cloned.1.call-done, bf16[2048,2816]{1,0:T(8,128)(2,1)} %all-gather.7.cloned.1.call-done), kind=kOutput, calls=%fused_computation.38 | convolution fusion | flops 5905580032 | bytes 19398656 | tf_op jit(solution)/shard_map/dot_general | solution.py:92
  241.0 0.0 copy-start.2
  241.0 81.9 %all-gather.11.cloned.1.call-done = bf16[2048,2816]{1,0:T(8,128)(2,1)} async-done(((bf16[128,2816]{1,0:T(8,128)(2,1)}), bf16[2048,2816]{1,0:T(8,128)(2,1)}) %all-gather.11.cloned.1.call-update) | async-done | bytes 11534352 | tf_op jit(solution)/shard_map/all_gather | solution.py:89
  322.9 94.4 %all-gather.9.cloned.1.call-done = bf16[2048,2816]{1,0:T(8,128)(2,1)} async-done(((bf16[128,2816]{1,0:T(8,128)(2,1)}), bf16[2048,2816]{1,0:T(8,128)(2,1)}) %all-gather.9.cloned.1.call-update) | async-done | bytes 11534352 | tf_op jit(solution)/shard_map/all_gather | solution.py:88
  417.3 27.3 %convolution_convert_fusion.1 = bf16[512,2048]{1,0:T(8,128)(2,1)} fusion(bf16[2048,2816]{1,0:T(8,128)(2,1)} %all-gather.11.cloned.1.call-done, f32[512,2816]{1,0:T(8,128)} %fusion.19, bf16[512,2048]{1,0:T(8,128)(2,1)} %all-gather.5.cloned.1.call-done, bf16[2048,2816]{1,0:T(8,128)(2,1)} %all-gather.9.cloned.1.call-done), kind=kOutput, calls=%fused_computation.11 | convolution fusion | flops 11820859392 | bytes 33030144 | tf_op jit(solution)/shard_map/dot_general | solution.py:96
  444.5 0.0 reduce-scatter.5.cloned.1.call-update
  444.6 30.3 %reduce-scatter.5.cloned.1.call-done = bf16[256,2048]{1,0:T(8,128)(2,1)} async-done(((bf16[512,2048]{1,0:T(8,128)(2,1)}), bf16[256,2048]{1,0:T(8,128)(2,1)}) %reduce-scatter.5.cloned.1.call-update) | async-done | bytes 1048592 | tf_op jit(solution)/shard_map/reduce_scatter | solution.py:95
  474.8 0.0 copy-done.2
  474.8 2.7 fusion.6
  (8 shorter events, 0.1 us)
Async XLA Ops:
  6.5 88.2 %reduce-scatter.3.cloned.1.call-start = ((), (), s32[]{:S(2)}) async-start(), calls=%async_computation.2 | async-start | bytes 3145728 | tf_op jit(solution)/shard_map/reduce_scatter | solution.py:72
  7.2 18.3 %collective-permute-start.2 = (bf16[128]{0:T(256)(128)(2,1)S(1)}, bf16[128]{0:T(256)(128)(2,1)S(1)}, u32[]{:S(2)}, u32[]{:S(2)}) collective-permute-start(bf16[128]{0:T(256)(128)(2,1)S(1)} %get-tuple-element.9), channel_id=1, source_target_pairs={{0,2},{2,4},{4,6},{6,8},{8,10},{10,12},{12,14},{14,16},{16,18},{18... | collective-permute-start | bytes 776 | tf_op jit(solution)/shard_map/ppermute | solution.py:19
  9.6 17.2 %collective-permute-start.3 = (bf16[128]{0:T(256)(128)(2,1)S(1)}, bf16[128]{0:T(256)(128)(2,1)S(1)}, u32[]{:S(2)}, u32[]{:S(2)}) collective-permute-start(bf16[128]{0:T(256)(128)(2,1)S(1)} %get-tuple-element.10), channel_id=1, source_target_pairs={{2,0},{4,2},{6,4},{8,6},{10,8},{12,10},{14,12},{16,14},{18,16},{20... | collective-permute-start | bytes 776 | tf_op jit(solution)/shard_map/ppermute | solution.py:20
  11.7 16.1 %collective-permute-start.4 = (bf16[128,128]{1,0:T(8,128)(2,1)S(1)}, bf16[128,128]{1,0:T(8,128)(2,1)S(1)}, u32[]{:S(2)}, u32[]{:S(2)}) collective-permute-start(bf16[128,128]{1,0:T(8,128)(2,1)S(1)} %get-tuple-element.5), channel_id=1, source_target_pairs={{0,2},{2,4},{4,6},{6,8},{8,10},{10,12},{12,14},{14,16},{16,18},{18... | collective-permute-start | bytes 98312 | tf_op jit(solution)/shard_map/ppermute | solution.py:19
  16.9 11.0 %collective-permute-start.5 = (bf16[128,128]{1,0:T(8,128)(2,1)S(1)}, bf16[128,128]{1,0:T(8,128)(2,1)S(1)}, u32[]{:S(2)}, u32[]{:S(2)}) collective-permute-start(bf16[128,128]{1,0:T(8,128)(2,1)S(1)} %get-tuple-element.6), channel_id=1, source_target_pairs={{2,0},{4,2},{6,4},{8,6},{10,8},{12,10},{14,12},{16,14},{18,16},{20... | collective-permute-start | bytes 98312 | tf_op jit(solution)/shard_map/ppermute | solution.py:20
  18.9 22.2 %collective-permute-start = (bf16[128,128]{1,0:T(8,128)(2,1)S(1)}, bf16[128,128]{1,0:T(8,128)(2,1)S(1)}, u32[]{:S(2)}, u32[]{:S(2)}) collective-permute-start(bf16[128,128]{1,0:T(8,128)(2,1)S(1)} %get-tuple-element.7), channel_id=1, source_target_pairs={{0,2},{2,4},{4,6},{6,8},{8,10},{10,12},{12,14},{14,16},{16,18},{18... | collective-permute-start | bytes 98312 | tf_op jit(solution)/shard_map/ppermute | solution.py:19
  25.5 15.6 %collective-permute-start.1 = (bf16[128,128]{1,0:T(8,128)(2,1)S(1)}, bf16[128,128]{1,0:T(8,128)(2,1)S(1)}, u32[]{:S(2)}, u32[]{:S(2)}) collective-permute-start(bf16[128,128]{1,0:T(8,128)(2,1)S(1)} %get-tuple-element.8), channel_id=1, source_target_pairs={{2,0},{4,2},{6,4},{8,6},{10,8},{12,10},{14,12},{16,14},{18,16},{20... | collective-permute-start | bytes 98312 | tf_op jit(solution)/shard_map/ppermute | solution.py:20
  32.7 8.4 %copy-start = (f32[2,768,512,8]{2,1,3,0:T(8,128)}, f32[2,768,512,8]{2,1,3,0:T(8,128)S(1)}, u32[]{:S(2)}) copy-start(f32[2,768,512,8]{2,1,3,0:T(8,128)S(1)} %get-tuple-element.12) | copy-start | bytes 75497472
  32.7 8.4 %copy-start.3 = (bf16[512,128]{1,0:T(8,128)(2,1)S(1)}, bf16[512,128]{1,0:T(8,128)(2,1)}, u32[]{:S(2)}) copy-start(bf16[512,128]{1,0:T(8,128)(2,1)} %param.14) | copy-start | bytes 393220
  41.3 12.0 %copy-start.5 = (bf16[1024,2048]{1,0:T(8,128)(2,1)S(1)}, bf16[1024,2048]{1,0:T(8,128)(2,1)}, u32[]{:S(2)}) copy-start(bf16[1024,2048]{1,0:T(8,128)(2,1)} %param.17) | copy-start | bytes 12582916
  53.4 3.9 copy-start.4
  53.4 41.3 %copy-start.1 = (bf16[256,2048]{1,0:T(8,128)(2,1)S(1)}, bf16[256,2048]{1,0:T(8,128)(2,1)}, u32[]{:S(2)}) copy-start(bf16[256,2048]{1,0:T(8,128)(2,1)} %param.11) | copy-start | bytes 3145732
  57.2 75.0 %all-gather.5.cloned.1.call-start = ((), (), s32[]{:S(2)}) async-start(), calls=%async_computation.3 | async-start | bytes 3145728 | tf_op jit(solution)/shard_map/all_gather | solution.py:91
  99.0 129.5 %all-gather.7.cloned.1.call-start = ((), (), s32[]{:S(2)}) async-start(), calls=%async_computation.4 | async-start | bytes 12255232 | tf_op jit(solution)/shard_map/all_gather | solution.py:87
  99.7 223.2 %all-gather.11.cloned.1.call-start = ((), (), s32[]{:S(2)}) async-start(), calls=%async_computation.6 | async-start | bytes 12255232 | tf_op jit(solution)/shard_map/all_gather | solution.py:89
  100.3 317.0 %all-gather.9.cloned.1.call-start = ((), (), s32[]{:S(2)}) async-start(), calls=%async_computation.5 | async-start | bytes 12255232 | tf_op jit(solution)/shard_map/all_gather | solution.py:88
  100.9 374.0 %reduce-scatter.5.cloned.1.call-start = ((), (), s32[]{:S(2)}) async-start(), calls=%async_computation.7 | async-start | bytes 3145728 | tf_op jit(solution)/shard_map/reduce_scatter | solution.py:95
  241.0 233.8 %copy-start.2 = (bf16[256,2048]{1,0:T(8,128)(2,1)S(1)}, bf16[256,2048]{1,0:T(8,128)(2,1)}, u32[]{:S(2)}) copy-start(bf16[256,2048]{1,0:T(8,128)(2,1)} %reduce-scatter.3.cloned.1.call-done) | copy-start | bytes 3145732
Sparse Core Ops, SparseCore 0:
  57.3 37.3 reduce-scatter.2
  99.1 33.0 all-gather.4
  134.5 93.9 all-gather.6
  230.7 92.2 all-gather.10
  325.0 92.2 all-gather.8
  444.7 30.1 reduce-scatter.4
where the time goes:
time: 485 us; the launch traced here: 484 us
  waiting for transfers between devices  373 us (77%)
  matrix products  59.3 us (12%)
  starting transfers between devices  16 us (3%)
  other arithmetic  15 us (3%)
  between operations  13.7 us (3%)
  local copies, waits for them, and re-layouts  7.17 us (1%)
    all_gather x1, waiting for transfers between devices, on_device(): lax.all_gather(gate_weight, 'sp', axis=0, tiled=True)  96.3 us
    all_gather x1, waiting for transfers between devices, on_device(): lax.all_gather(up_weight, 'sp', axis=0, tiled=True)  94.4 us
    all_gather x1, waiting for transfers between devices, on_device(): lax.all_gather(down_weight, 'sp', axis=0, tiled=True)  81.9 us
    reduce_scatter x1, waiting for transfers between devices, on_device(): lax.psum_scatter(jnp.dot(attended, out_weight, preferred_element_type=jnp...  37.5 us
    all_gather x1, waiting for transfers between devices, on_device(): row_piece = lax.all_gather(normed, 'tp', axis=0, tiled=True)  31.3 us
    reduce_scatter x1, waiting for transfers between devices, on_device(): lax.psum_scatter(lax.dot_general(hidden, whole_down, (((1,), (1,)), ((),...  30.3 us
    dot_general x1, matrix products, on_device(): lax.dot_general(hidden, whole_down, (((1,), (1,)), ((), ())), preferred_e...  27.3 us
    dot_general x1, matrix products, on_device(): jnp.dot(row_piece, whole_gate, preferred_element_type=jnp.float32)  12.5 us
  transfers between devices with their start and end apart: 12, of which 6 were waited for; matrix products, arithmetic and copies ran while one was open for 6% of the time, Pallas kernels for 0%

commit v1 on v0

--- a/solution.py
+++ b/solution.py
@@ -84,7 +84,9 @@
     )
     normed = (scaled * norm_gain.astype(jnp.float32)).astype(jnp.bfloat16)
     whole_gate, whole_up, whole_down = (
-        lax.all_gather(gate_weight, "sp", axis=0, tiled=True),
+        jnp.concatenate(
+            lax.all_to_all(jnp.stack([gate_weight] * lax.axis_size("sp")), "sp", 0, 0), axis=0
+        ),
         lax.all_gather(up_weight, "sp", axis=0, tiled=True),
         lax.all_gather(down_weight, "sp", axis=0, tiled=True),
     )

time: 485 us -> 577 us (1.19)
  waiting for transfers between devices: 373 us -> 454 us
    all_to_all x0 -> x1, waiting for transfers between devices: none -> 253 us  [on_device(): lax.all_to_all(jnp.stack([gate_weight] * lax.axis_size('sp')), 'sp', 0, 0)]
    all_gather x1 -> x0, waiting for transfers between devices: 96.3 us -> none  [on_device(): lax.all_gather(gate_weight, 'sp', axis=0, tiled=True)]
    all_gather x1, waiting for transfers between devices: 94.4 us -> 0.01 us  [on_device(): lax.all_gather(up_weight, 'sp', axis=0, tiled=True)]
    all_gather x1, waiting for transfers between devices: 81.9 us -> 105 us  [on_device(): lax.all_gather(down_weight, 'sp', axis=0, tiled=True)]
    all_gather x1, waiting for transfers between devices: 31.3 us -> 20.9 us  [on_device(): row_piece = lax.all_gather(normed, 'tp', axis=0, tiled=True)]
    reduce_scatter x1, waiting for transfers between devices: 30.3 us -> 36.3 us  [on_device(): lax.psum_scatter(lax.dot_general(hidden, whole_down, (((1,), (1,)), ((),...]
  transfers between devices with their start and end apart: 12 -> 12, of which waited for: 6 -> 5; matrix products, arithmetic and copies ran while one was open for 6% -> 6% of each run, Pallas kernels for 0% -> 0%
where the time goes in v1:
time: 577 us; the launch traced here: 576 us
  waiting for transfers between devices  454 us (79%)
  matrix products  59.7 us (10%)
  starting transfers between devices  21.6 us (4%)
  other arithmetic  15 us (3%)
  between operations  13.4 us (2%)
  local copies, waits for them, and re-layouts  12.4 us (2%)
    all_to_all x1, waiting for transfers between devices, on_device(): lax.all_to_all(jnp.stack([gate_weight] * lax.axis_size('sp')), 'sp', 0, 0)  253 us
    all_gather x1, waiting for transfers between devices, on_device(): lax.all_gather(down_weight, 'sp', axis=0, tiled=True)  105 us
    reduce_scatter x1, waiting for transfers between devices, on_device(): lax.psum_scatter(jnp.dot(attended, out_weight, preferred_element_type=jnp...  37.5 us
    reduce_scatter x1, waiting for transfers between devices, on_device(): lax.psum_scatter(lax.dot_general(hidden, whole_down, (((1,), (1,)), ((),...  36.3 us
    dot_general x1, matrix products, on_device(): lax.dot_general(hidden, whole_down, (((1,), (1,)), ((), ())), preferred_e...  27.2 us
    all_gather x1, waiting for transfers between devices, on_device(): row_piece = lax.all_gather(normed, 'tp', axis=0, tiled=True)  20.9 us
    dot_general x1, matrix products, on_device(): jnp.dot(row_piece, whole_gate, preferred_element_type=jnp.float32)  12.9 us
    dot_general x1, matrix products, on_device(): jnp.einsum('kgqj,jkd->qkgd', probs, value_block, preferred_element_type=j...  12 us
  transfers between devices with their start and end apart: 12, of which 5 were waited for; matrix products, arithmetic and copies ran while one was open for 6% of the time, Pallas kernels for 0%

profile of v1, /device:TPU:0, one launch (start us, length us, event | category | flops | bytes accessed | tf_op | source)
XLA Modules:
  0.0 576.1 jit_solution(10580042087553921983)
XLA Ops:
  6.5 0.0 reduce-scatter.3.cloned.1.call-start
  6.5 0.7 convert_element_type.50
  7.2 2.4 collective-permute-start.2
  9.6 1.3 collective-permute-start.3
  10.9 0.8 fusion.16
  11.7 5.1 collective-permute-start.4
  16.9 1.3 collective-permute-start.5
  18.2 0.8 fusion.17
  18.9 4.3 collective-permute-start
  23.3 1.5 copy.18
  24.8 0.7 max.17
  25.5 0.0 collective-permute-done.2
  25.5 1.3 collective-permute-start.1
  26.8 0.0 collective-permute-done.3
  26.8 1.0 fusion.9
  27.8 0.0 collective-permute-done.4
  27.8 0.0 collective-permute-done.5
  27.8 0.9 pad_maximum_fusion.1
  28.8 0.1 copy.17
  28.9 3.7 fusion.1
  32.7 0.0 copy-start
  32.7 0.1 broadcast_maximum_fusion
  32.7 0.0 copy-start.4
  32.7 5.2 fusion
  38.0 3.0 copy-done
  41.0 0.1 exponential_add_fusion
  41.1 0.0 collective-permute-done
  41.1 0.0 collective-permute-done.1
  41.1 0.0 copy-done.4
  41.2 0.1 copy.16
  41.3 0.0 copy-start.6
  41.3 12.0 %fusion.10 = bf16[2,64,8,512]{3,1,2,0:T(8,128)(2,1)S(1)} fusion(bf16[768,2,64,1]{0,2,3,1:T(8,128)(2,1)S(1)} %bitcast.38, f32[2,768,512,8]{2,1,3,0:T(8,128)} %copy-done, f32[2,8,512]{2,1,0:T(8,128)S(1)} %exponential_add_fusion, f32[2,8,512]{2,1,0:T(8,128)S(1)} %broadcast_maximum_fusion, pred[512,768]{0,1:T(8,128)(4,1)S(1)} %fusion.9), kind=kOutput, calls=%fused_computation.21 | convolution fusion | flops 837287936 | bytes 26869760 | tf_op jit(solution)/shard_map/kgqj,jkd->qkgd/dot_general | solution.py:70
  53.3 0.0 copy-done.6
  53.4 0.0 copy-start.5
  53.4 0.0 copy-start.1
  53.4 3.8 convolution_convert_fusion
  57.2 0.0 copy-start.3
  57.2 0.0 reduce-scatter.3.cloned.1.call-update
  57.2 0.0 all-gather.4.cloned.1.call-start
  57.2 0.0 copy-done.5
  57.3 37.5 %reduce-scatter.3.cloned.1.call-done = bf16[256,2048]{1,0:T(8,128)(2,1)} async-done(((bf16[512,2048]{1,0:T(8,128)(2,1)}), bf16[256,2048]{1,0:T(8,128)(2,1)}) %reduce-scatter.3.cloned.1.call-update) | async-done | bytes 1048592 | tf_op jit(solution)/shard_map/reduce_scatter | solution.py:72
  94.7 0.0 copy-done.1
  94.7 1.6 fusion.3
  96.4 2.6 fusion.5
  99.0 0.0 all-gather.4.cloned.1.call-update
  99.0 0.2 all-gather.6.cloned.1.call-start
  99.2 0.5 all-gather.6.cloned.1.call-update
  99.7 0.0 copy-done.3
  99.7 5.3 stack.2
  105.0 5.7 all-to-all-start
  110.7 0.0 all-gather.8.cloned.1.call-start
  110.7 0.5 all-gather.8.cloned.1.call-update
  111.2 0.0 reduce-scatter.5.cloned.1.call-start
  111.3 20.9 %all-gather.4.cloned.1.call-done = bf16[512,2048]{1,0:T(8,128)(2,1)} async-done(((bf16[256,2048]{1,0:T(8,128)(2,1)}), bf16[512,2048]{1,0:T(8,128)(2,1)}) %all-gather.4.cloned.1.call-update) | async-done | bytes 2097168 | tf_op jit(solution)/shard_map/all_gather | solution.py:93
  132.2 253.4 %all-to-all-done = bf16[16,128,2816]{2,1,0:T(8,128)(2,1)} async-done(((bf16[16,128,2816]{2,1,0:T(8,128)(2,1)}), bf16[16,128,2816]{2,1,0:T(8,128)(2,1)}, u32[]{:S(2)}, u32[]{:S(2)}) %all-to-all-start) | async-done | bytes 11534368 | tf_op jit(solution)/shard_map/all_to_all | solution.py:88
  385.6 12.9 %fusion.19 = f32[512,2816]{1,0:T(8,128)} fusion(bf16[512,2048]{1,0:T(8,128)(2,1)} %all-gather.4.cloned.1.call-done, bf16[2048,2816]{1,0:T(8,128)(2,1)} %bitcast.10), kind=kOutput, calls=%fused_computation.38 | convolution fusion | flops 5905580032 | bytes 19398656 | tf_op jit(solution)/shard_map/dot_general | solution.py:94
  398.5 0.0 copy-start.2
  398.5 0.0 all-gather.6.cloned.1.call-done
  398.5 104.8 %all-gather.8.cloned.1.call-done = bf16[2048,2816]{1,0:T(8,128)(2,1)} async-done(((bf16[128,2816]{1,0:T(8,128)(2,1)}), bf16[2048,2816]{1,0:T(8,128)(2,1)}) %all-gather.8.cloned.1.call-update) | async-done | bytes 11534352 | tf_op jit(solution)/shard_map/all_gather | solution.py:91
  503.2 27.2 %convolution_convert_fusion.1 = bf16[512,2048]{1,0:T(8,128)(2,1)} fusion(bf16[2048,2816]{1,0:T(8,128)(2,1)} %all-gather.8.cloned.1.call-done, f32[512,2816]{1,0:T(8,128)} %fusion.19, bf16[512,2048]{1,0:T(8,128)(2,1)} %all-gather.4.cloned.1.call-done, bf16[2048,2816]{1,0:T(8,128)(2,1)} %all-gather.6.cloned.1.call-done), kind=kOutput, calls=%fused_computation.11 | convolution fusion | flops 11820859392 | bytes 33030144 | tf_op jit(solution)/shard_map/dot_general | solution.py:98
  530.5 0.0 reduce-scatter.5.cloned.1.call-update
  530.5 36.3 %reduce-scatter.5.cloned.1.call-done = bf16[256,2048]{1,0:T(8,128)(2,1)} async-done(((bf16[512,2048]{1,0:T(8,128)(2,1)}), bf16[256,2048]{1,0:T(8,128)(2,1)}) %reduce-scatter.5.cloned.1.call-update) | async-done | bytes 1048592 | tf_op jit(solution)/shard_map/reduce_scatter | solution.py:97
  566.8 0.0 copy-done.2
  566.8 2.7 fusion.6
  (8 shorter events, 0.1 us)
Async XLA Ops:
  6.5 88.2 %reduce-scatter.3.cloned.1.call-start = ((), (), s32[]{:S(2)}) async-start(), calls=%async_computation.3 | async-start | bytes 3145728 | tf_op jit(solution)/shard_map/reduce_scatter | solution.py:72
  7.2 18.3 %collective-permute-start.2 = (bf16[128]{0:T(256)(128)(2,1)S(1)}, bf16[128]{0:T(256)(128)(2,1)S(1)}, u32[]{:S(2)}, u32[]{:S(2)}) collective-permute-start(bf16[128]{0:T(256)(128)(2,1)S(1)} %get-tuple-element.9), channel_id=1, source_target_pairs={{0,2},{2,4},{4,6},{6,8},{8,10},{10,12},{12,14},{14,16},{16,18},{18... | collective-permute-start | bytes 776 | tf_op jit(solution)/shard_map/ppermute | solution.py:19
  9.6 17.2 %collective-permute-start.3 = (bf16[128]{0:T(256)(128)(2,1)S(1)}, bf16[128]{0:T(256)(128)(2,1)S(1)}, u32[]{:S(2)}, u32[]{:S(2)}) collective-permute-start(bf16[128]{0:T(256)(128)(2,1)S(1)} %get-tuple-element.10), channel_id=1, source_target_pairs={{2,0},{4,2},{6,4},{8,6},{10,8},{12,10},{14,12},{16,14},{18,16},{20... | collective-permute-start | bytes 776 | tf_op jit(solution)/shard_map/ppermute | solution.py:20
  11.7 16.1 %collective-permute-start.4 = (bf16[128,128]{1,0:T(8,128)(2,1)S(1)}, bf16[128,128]{1,0:T(8,128)(2,1)S(1)}, u32[]{:S(2)}, u32[]{:S(2)}) collective-permute-start(bf16[128,128]{1,0:T(8,128)(2,1)S(1)} %get-tuple-element.5), channel_id=1, source_target_pairs={{0,2},{2,4},{4,6},{6,8},{8,10},{10,12},{12,14},{14,16},{16,18},{18... | collective-permute-start | bytes 98312 | tf_op jit(solution)/shard_map/ppermute | solution.py:19
  16.9 11.0 %collective-permute-start.5 = (bf16[128,128]{1,0:T(8,128)(2,1)S(1)}, bf16[128,128]{1,0:T(8,128)(2,1)S(1)}, u32[]{:S(2)}, u32[]{:S(2)}) collective-permute-start(bf16[128,128]{1,0:T(8,128)(2,1)S(1)} %get-tuple-element.6), channel_id=1, source_target_pairs={{2,0},{4,2},{6,4},{8,6},{10,8},{12,10},{14,12},{16,14},{18,16},{20... | collective-permute-start | bytes 98312 | tf_op jit(solution)/shard_map/ppermute | solution.py:20
  18.9 22.2 %collective-permute-start = (bf16[128,128]{1,0:T(8,128)(2,1)S(1)}, bf16[128,128]{1,0:T(8,128)(2,1)S(1)}, u32[]{:S(2)}, u32[]{:S(2)}) collective-permute-start(bf16[128,128]{1,0:T(8,128)(2,1)S(1)} %get-tuple-element.7), channel_id=1, source_target_pairs={{0,2},{2,4},{4,6},{6,8},{8,10},{10,12},{12,14},{14,16},{16,18},{18... | collective-permute-start | bytes 98312 | tf_op jit(solution)/shard_map/ppermute | solution.py:19
  25.5 15.6 %collective-permute-start.1 = (bf16[128,128]{1,0:T(8,128)(2,1)S(1)}, bf16[128,128]{1,0:T(8,128)(2,1)S(1)}, u32[]{:S(2)}, u32[]{:S(2)}) collective-permute-start(bf16[128,128]{1,0:T(8,128)(2,1)S(1)} %get-tuple-element.8), channel_id=1, source_target_pairs={{2,0},{4,2},{6,4},{8,6},{10,8},{12,10},{14,12},{16,14},{18,16},{20... | collective-permute-start | bytes 98312 | tf_op jit(solution)/shard_map/ppermute | solution.py:20
  32.7 8.4 %copy-start = (f32[2,768,512,8]{2,1,3,0:T(8,128)}, f32[2,768,512,8]{2,1,3,0:T(8,128)S(1)}, u32[]{:S(2)}) copy-start(f32[2,768,512,8]{2,1,3,0:T(8,128)S(1)} %get-tuple-element.12) | copy-start | bytes 75497472
  32.7 8.4 %copy-start.4 = (bf16[512,128]{1,0:T(8,128)(2,1)S(1)}, bf16[512,128]{1,0:T(8,128)(2,1)}, u32[]{:S(2)}) copy-start(bf16[512,128]{1,0:T(8,128)(2,1)} %param.14) | copy-start | bytes 393220
  41.3 12.0 %copy-start.6 = (bf16[1024,2048]{1,0:T(8,128)(2,1)S(1)}, bf16[1024,2048]{1,0:T(8,128)(2,1)}, u32[]{:S(2)}) copy-start(bf16[1024,2048]{1,0:T(8,128)(2,1)} %param.17) | copy-start | bytes 12582916
  53.4 3.9 copy-start.5
  53.4 41.3 %copy-start.1 = (bf16[256,2048]{1,0:T(8,128)(2,1)S(1)}, bf16[256,2048]{1,0:T(8,128)(2,1)}, u32[]{:S(2)}) copy-start(bf16[256,2048]{1,0:T(8,128)(2,1)} %param.11) | copy-start | bytes 3145732
  57.2 42.6 %copy-start.3 = (bf16[128,2816]{1,0:T(8,128)(2,1)S(1)}, bf16[128,2816]{1,0:T(8,128)(2,1)}, u32[]{:S(2)}) copy-start(bf16[128,2816]{1,0:T(8,128)(2,1)} %param.19) | copy-start | bytes 2162692
  57.2 75.0 %all-gather.4.cloned.1.call-start = ((), (), s32[]{:S(2)}) async-start(), calls=%async_computation.4 | async-start | bytes 3145728 | tf_op jit(solution)/shard_map/all_gather | solution.py:93
  99.0 299.5 %all-gather.6.cloned.1.call-start = ((), (), s32[]{:S(2)}) async-start(), calls=%async_computation.5 | async-start | bytes 12255232 | tf_op jit(solution)/shard_map/all_gather | solution.py:90
  105.0 280.6 %all-to-all-start = ((bf16[16,128,2816]{2,1,0:T(8,128)(2,1)}), bf16[16,128,2816]{2,1,0:T(8,128)(2,1)}, u32[]{:S(2)}, u32[]{:S(2)}) async-start(bf16[16,128,2816]{2,1,0:T(8,128)(2,1)} %stack.2), calls=%async_computation.1 | async-start | bytes 23068672 | tf_op jit(solution)/shard_map/all_to_all | solution.py:88
  110.7 392.6 %all-gather.8.cloned.1.call-start = ((), (), s32[]{:S(2)}) async-start(), calls=%async_computation.6 | async-start | bytes 12255232 | tf_op jit(solution)/shard_map/all_gather | solution.py:91
  111.2 455.6 %reduce-scatter.5.cloned.1.call-start = ((), (), s32[]{:S(2)}) async-start(), calls=%async_computation.7 | async-start | bytes 3145728 | tf_op jit(solution)/shard_map/reduce_scatter | solution.py:97
  398.5 168.3 %copy-start.2 = (bf16[256,2048]{1,0:T(8,128)(2,1)S(1)}, bf16[256,2048]{1,0:T(8,128)(2,1)}, u32[]{:S(2)}) copy-start(bf16[256,2048]{1,0:T(8,128)(2,1)} %reduce-scatter.3.cloned.1.call-done) | copy-start | bytes 3145732
Sparse Core Ops, SparseCore 0:
  57.3 37.3 reduce-scatter.2
  99.1 33.0 all-gather.3
  134.5 230.4 all-gather.5
  367.1 136.0 all-gather.7
  530.6 36.1 reduce-scatter.4
